TPU v7x, 32 devices: a whole 2x2x4 slice. The times are simulated.
32 devices in a mesh: ep: 8 (over z, y), tp: 4 (over x, core).
Axes of the slice: x: 2, y: 2, z: 4, core: 2. Of those that a mesh axis runs over, the one named last changes fastest.
Arguments:
- queries: bfloat16 [4096, 1024], P('ep', 'tp'), may hold values from -6 to 6
- keys: bfloat16 [4096, 512], P('ep', 'tp'), may hold values from -6 to 6
- values: bfloat16 [4096, 512], P('ep', 'tp'), may hold values from -384 to 384
- query_gain: float32 [128], replicated, may hold values from 0.1 to 1.9
- key_gain: float32 [128], replicated, may hold values from 0.1 to 1.9
- out_proj: bfloat16 [1024, 2048], replicated, may hold values from -0.1875 to 0.1875
- tokens_b: bfloat16 [4096, 2048], P(('ep', 'tp')), may hold values from -6 to 6
- norm_gain: float32 [2048], replicated, may hold values from 0.1 to 1.9
- routes: int32 [4096, 2], P(('ep', 'tp')), may hold values from 0 to 31, all different within a row; in each aligned block of 128 rows (0 to 127, 128 to 255, ...) at most 16 rows name the same one
- group_prob: float32 [4096], P(('ep', 'tp')), may hold values from 0.25 to 1
- expert_logits: float32 [4096, 2], P(('ep', 'tp')), may hold values from -6 to 6
- w_gate: bfloat16 [32, 2048, 512], P(('ep', 'tp')), may hold values from -0.125 to 0.125
- w_up: bfloat16 [32, 2048, 512], P(('ep', 'tp')), may hold values from -0.125 to 0.125
- w_down: bfloat16 [32, 512, 2048], P(('ep', 'tp')), may hold values from -0.25 to 0.25
Outputs:
- mixed_a: bfloat16 [4096, 2048], P(('ep', 'tp'))
- mixed_b: bfloat16 [4096, 2048], P(('ep', 'tp'))
Inputs may be any that keep to these rules, and one draw needn't show every extreme that they name: Within the 128 rows of one device, no expert is named by more than 16 of the routes, and in every draw some expert is named exactly 16 times by the rows of some device. The 2 experts of a row differ.
All inputs are finite; a program needn't handle non-finite values.
Results may differ from a plain program's by a relative error of at most 0.014.
Values may be sent and summed in bfloat16 or wider, within the bound.
A program may use at most 128 MiB of HBM per device.

v0:
```python
import math
import jax
import jax.numpy as jnp
from jax import lax
from jax.sharding import PartitionSpec as P

GRID_W = 64
NORM_EPS = 1e-06
ROPE_BASE = 10000.0


def rope_angles(row_count, offset, head_dim):
    quarter = head_dim // 4
    position = offset + jnp.arange(row_count, dtype=jnp.int32)
    grid_row = (position // GRID_W).astype(jnp.float32)
    grid_col = (position % GRID_W).astype(jnp.float32)
    frequency = ROPE_BASE ** (-jnp.arange(quarter, dtype=jnp.float32) / quarter)
    angles = jnp.concatenate([grid_row[:, None] * frequency, grid_col[:, None] * frequency], axis=1)
    return (jnp.cos(angles), jnp.sin(angles))


def norm_rotate(block_in, gain, cos_table, sin_table):
    wide = block_in.astype(jnp.float32)
    wide = wide * lax.rsqrt(jnp.mean(wide * wide, axis=-1, keepdims=True) + NORM_EPS) * gain
    half_width = wide.shape[-1] // 2
    first_half, second_half = (wide[..., :half_width], wide[..., half_width:])
    cos_b = cos_table[:, None, :]
    sin_b = sin_table[:, None, :]
    turned = jnp.concatenate(
        [first_half * cos_b - second_half * sin_b, second_half * cos_b + first_half * sin_b],
        axis=-1,
    )
    return turned.astype(jnp.bfloat16)


def attention_half(queries, keys, values, query_gain, key_gain, out_proj):
    row_count = queries.shape[0]
    head_dim = query_gain.shape[0]
    local_heads = queries.shape[1] // head_dim
    local_kv = keys.shape[1] // head_dim
    group_size = local_heads // local_kv
    offset = lax.axis_index("ep") * row_count
    cos_table, sin_table = rope_angles(row_count, offset, head_dim)
    qrot = norm_rotate(
        queries.reshape(row_count, local_heads, head_dim), query_gain, cos_table, sin_table
    )
    qrot = qrot.reshape(row_count, local_kv, group_size, head_dim)
    krot = norm_rotate(keys.reshape(row_count, local_kv, head_dim), key_gain, cos_table, sin_table)
    krot = krot.reshape(row_count, local_kv * head_dim)
    score_scale = head_dim ** (-0.5)
    start_pair = (
        jnp.zeros((row_count, local_kv, group_size, head_dim), jnp.float32),
        jnp.zeros((row_count, local_kv, group_size), jnp.float32),
    )
    key_piece = lax.all_gather(krot, "ep", axis=0, tiled=True)
    value_piece = lax.all_gather(values, "ep", axis=0, tiled=True)
    piece_rows = key_piece.shape[0]
    key_block = math.gcd(piece_rows, 1024)
    block_count = piece_rows // key_block
    key_tiles = key_piece.reshape(block_count, key_block, local_kv, head_dim)
    value_tiles = value_piece.reshape(block_count, key_block, local_kv, head_dim)

    def key_step(pair, tiles):
        numerator, denominator = pair
        key_tile, value_tile = tiles
        scores = (
            jnp.einsum("qhgd,khd->qhgk", qrot, key_tile, preferred_element_type=jnp.float32)
            * score_scale
        )
        weights = jnp.exp(scores).astype(jnp.bfloat16)
        denominator = denominator + jnp.sum(weights.astype(jnp.float32), axis=-1)
        numerator = numerator + jnp.einsum(
            "qhgk,khd->qhgd", weights, value_tile, preferred_element_type=jnp.float32
        )
        return ((numerator, denominator), None)

    numerator, denominator = lax.scan(key_step, start_pair, (key_tiles, value_tiles))[0]
    attended = (
        (numerator / denominator[..., None])
        .astype(jnp.bfloat16)
        .reshape(row_count, local_heads * head_dim)
    )
    own_width = local_heads * head_dim
    own_rows = lax.dynamic_slice_in_dim(out_proj, lax.axis_index("tp") * own_width, own_width, 0)
    return lax.psum_scatter(
        jnp.dot(attended, own_rows, preferred_element_type=jnp.float32).astype(jnp.bfloat16),
        "tp",
        scatter_dimension=0,
        tiled=True,
    )


def expert_apply(inputs, gate_w, up_w, down_w):
    gate_part = jnp.dot(inputs, gate_w, preferred_element_type=jnp.float32)
    up_part = jnp.dot(inputs, up_w, preferred_element_type=jnp.float32)
    hidden = (jax.nn.silu(gate_part) * up_part).astype(jnp.bfloat16)
    return jnp.dot(hidden, down_w, preferred_element_type=jnp.float32).astype(jnp.bfloat16)


def expert_half(tokens_b, norm_gain, routes, group_prob, expert_logits, w_gate, w_up, w_down):
    ep_count = lax.axis_size("ep")
    tp_count = lax.axis_size("tp")
    device_count = ep_count * tp_count
    row_count, top_count = routes.shape
    model_width = tokens_b.shape[1]
    capacity = 2 * top_count * row_count // device_count
    wide_b = tokens_b.astype(jnp.float32)
    normed = (
        wide_b * lax.rsqrt(jnp.mean(wide_b * wide_b, axis=-1, keepdims=True) + NORM_EPS) * norm_gain
    ).astype(jnp.bfloat16)
    flat_routes = routes.reshape(-1)
    onehot = (flat_routes[:, None] == jnp.arange(device_count, dtype=jnp.int32)[None, :]).astype(
        jnp.int32
    )
    slot_rank = jnp.sum((jnp.cumsum(onehot, axis=0) - onehot) * onehot, axis=1)
    target_slot = flat_routes * capacity + slot_rank
    token_index = jnp.arange(row_count * top_count, dtype=jnp.int32) // top_count
    sender = (
        jnp.zeros((device_count * capacity, model_width), jnp.bfloat16)
        .at[target_slot]
        .set(normed[token_index])
    )
    arrived = lax.all_to_all(
        sender.reshape(device_count, capacity, model_width),
        ("ep", "tp"),
        split_axis=0,
        concat_axis=0,
        tiled=True,
    )
    expert_out = expert_apply(
        arrived.reshape(device_count * capacity, model_width), w_gate[0], w_up[0], w_down[0]
    )
    returned = lax.all_to_all(
        expert_out.reshape(device_count, capacity, model_width),
        ("ep", "tp"),
        split_axis=0,
        concat_axis=0,
        tiled=True,
    )
    returned = returned.reshape(device_count * capacity, model_width)
    picked = returned[target_slot].reshape(row_count, top_count, model_width).astype(jnp.float32)
    combine = group_prob[:, None] * jax.nn.softmax(expert_logits, axis=-1)
    return jnp.sum(picked * combine[:, :, None], axis=1).astype(jnp.bfloat16)


def body(
    queries,
    keys,
    values,
    query_gain,
    key_gain,
    out_proj,
    tokens_b,
    norm_gain,
    routes,
    group_prob,
    expert_logits,
    w_gate,
    w_up,
    w_down,
):
    mixed_a = attention_half(queries, keys, values, query_gain, key_gain, out_proj)
    mixed_b = expert_half(
        tokens_b, norm_gain, routes, group_prob, expert_logits, w_gate, w_up, w_down
    )
    return (mixed_a, mixed_b)


def solution(mesh):
    placed = (
        P("ep", "tp"),
        P("ep", "tp"),
        P("ep", "tp"),
        P(),
        P(),
        P(),
        P(("ep", "tp"), None),
        P(),
        P(("ep", "tp"), None),
        P(("ep", "tp")),
        P(("ep", "tp"), None),
        P(("ep", "tp"), None, None),
        P(("ep", "tp"), None, None),
        P(("ep", "tp"), None, None),
    )
    return jax.shard_map(
        body,
        mesh=mesh,
        in_specs=placed,
        out_specs=(P(("ep", "tp"), None), P(("ep", "tp"), None)),
        check_vma=False,
    )
```

profile of v0, /device:TPU:0, one launch (start us, length us, event | category | flops | bytes accessed | tf_op | source)
XLA Modules:
  0.0 214.3 jit_solution(13210312035628791452)
XLA Ops:
  7.3 1.2 copy.30
  8.5 0.7 fusion.40
  9.3 0.1 broadcast_multiply_fusion.1
  9.4 0.5 fusion.47
  9.9 0.7 pad_maximum_fusion.2
  10.6 0.7 all-gather.3.cloned.1.call-update
  11.3 0.1 copy.36
  11.4 0.1 eq.31
  11.6 0.1 eq.27
  11.7 0.6 reduce-window.6
  12.3 0.2 slice_reduce_fusion
  12.6 0.1 copy.35
  12.7 0.1 mul.229
  12.8 0.2 fusion.26
  13.0 0.1 fusion.51
  13.2 0.2 fusion.28
  13.4 7.0 %scatter_custom_fusion = bf16[512,2048]{1,0:T(8,128)(2,1)} fusion(s32[256]{0:T(256)S(1)} %bitcast.124, bf16[128,2048]{1,0:T(8,128)(2,1)S(1)} %fusion.28, s32[1024]{0:T(1024)S(1)} %pad_clamp_fusion.1, bf16[]{:T(256)} %constant.102.clone.1), kind=kCustom, calls=%fused_computation.32 | custom fusion | bytes 2097154 | tf_op jit(solution)/shard_map/scatter | solution.py:121
  20.4 7.6 %all-to-all-start = ((bf16[32,16,2048]{2,1,0:T(8,128)(2,1)}), bf16[32,16,2048]{2,1,0:T(8,128)(2,1)}, u32[]{:S(2)}, u32[]{:S(2)}) async-start(bf16[32,16,2048]{2,1,0:T(8,128)(2,1)} %bitcast.118), calls=%async_computation.1 | async-start | bytes 4194304 | tf_op jit(solution)/shard_map/all_to_all | solution.py:123
  28.0 0.1 copy.31
  28.2 0.5 fusion.44
  28.7 0.1 fusion.35
  28.8 0.1 fusion.36
  28.9 0.1 fusion.41
  29.0 0.2 copy.34
  29.2 39.7 %all-gather.5.cloned.1.call-done = bf16[4096,128]{0,1:T(8,128)(2,1)} async-done(((bf16[512,128]{0,1:T(8,128)(2,1)}), bf16[4096,128]{0,1:T(8,128)(2,1)}) %all-gather.5.cloned.1.call-update) | async-done | bytes 1048592 | tf_op jit(solution)/shard_map/all_gather | solution.py:55
  68.8 2.3 %copy.41 = bf16[4096,128]{1,0:T(8,128)(2,1)} copy(bf16[4096,128]{0,1:T(8,128)(2,1)} %all-gather.5.cloned.1.call-done) | data formatting | bytes 2097152
  71.1 40.1 %all-gather.3.cloned.1.call-done = bf16[4096,128]{1,0:T(8,128)(2,1)} async-done(((bf16[512,128]{1,0:T(8,128)(2,1)}), bf16[4096,128]{1,0:T(8,128)(2,1)}) %all-gather.3.cloned.1.call-update) | async-done | bytes 1048592 | tf_op jit(solution)/shard_map/all_gather | solution.py:56
  111.2 21.3 %while.13 = (s32[]{:T(128)}, f32[512,1,2,128]{0,3,2,1:T(8,128)S(1)}, f32[512,1,2]{0,2,1:T(2,128)S(1)}, bf16[4,1024,1,128]{3,1,0,2:T(8,128)(2,1)}, bf16[4,1024,1,...) while((s32[]{:T(128)}, ...), condition=%wide.region_4.5_spmd.clone, body=%wide.region_2.4_spmd.clone.sunk | while | flops 541328384 | bytes 6046816 | solution.py:77
  111.2 3.1 %convert_reduce_fusion.2 = (f32[512,2]{0,1:T(2,128)S(1)}, bf16[1024,512,2]{1,0,2:T(8,128)(2,1)}) fusion(bf16[512,1,2,128]{3,0,2,1:T(8,128)(2,1)S(1)} %get-tuple-element.160, bf16[4,1024,1,128]{3,1,2,0:T(8,128)(2,1)} %get-tuple-element.159, s32[]{:T(128)} %get-tuple-element.147), kind=kOutput, calls=%fused_computation.3.clone.1 | convolution fusion | flops 272628736 | bytes 2626048 | tf_op jit(solution)/shard_map/while/body/eval_jaxpr/qhgd,khd->qhgk/dot_general | solution.py:67
  114.3 2.2 %fusion.71 = f32[512,1,2,128]{0,3,2,1:T(8,128)S(1)} fusion(bf16[1024,512,2]{1,0,2:T(8,128)(2,1)} %get-tuple-element.137, f32[512,1,2,128]{0,3,2,1:T(8,128)S(1)} %get-tuple-element.148, bf16[4,1024,1,128]{3,1,0,2:T(8,128)(2,1)} %get-tuple-element.158, s32[]{:T(128)} %get-tuple-element.147, pred[]{:T(512)S(6)} %compare.18), kind=kOutput, calls=%fused_computation.8.clone.1 | convolution fusion | flops 268697600 | bytes 3408385 | tf_op jit(solution)/shard_map/while/body/eval_jaxpr/qhgk,khd->qhgd/dot_general | solution.py:72
  116.6 3.1 %convert_reduce_fusion.2 = (f32[512,2]{0,1:T(2,128)S(1)}, bf16[1024,512,2]{1,0,2:T(8,128)(2,1)}) fusion(bf16[512,1,2,128]{3,0,2,1:T(8,128)(2,1)S(1)} %get-tuple-element.160, bf16[4,1024,1,128]{3,1,2,0:T(8,128)(2,1)} %get-tuple-element.159, s32[]{:T(128)} %get-tuple-element.147), kind=kOutput, calls=%fused_computation.3.clone.1 | convolution fusion | flops 272628736 | bytes 2626048 | tf_op jit(solution)/shard_map/while/body/eval_jaxpr/qhgd,khd->qhgk/dot_general | solution.py:67
  119.7 2.2 %fusion.71 = f32[512,1,2,128]{0,3,2,1:T(8,128)S(1)} fusion(bf16[1024,512,2]{1,0,2:T(8,128)(2,1)} %get-tuple-element.137, f32[512,1,2,128]{0,3,2,1:T(8,128)S(1)} %get-tuple-element.148, bf16[4,1024,1,128]{3,1,0,2:T(8,128)(2,1)} %get-tuple-element.158, s32[]{:T(128)} %get-tuple-element.147, pred[]{:T(512)S(6)} %compare.18), kind=kOutput, calls=%fused_computation.8.clone.1 | convolution fusion | flops 268697600 | bytes 3408385 | tf_op jit(solution)/shard_map/while/body/eval_jaxpr/qhgk,khd->qhgd/dot_general | solution.py:72
  121.9 3.1 %convert_reduce_fusion.2 = (f32[512,2]{0,1:T(2,128)S(1)}, bf16[1024,512,2]{1,0,2:T(8,128)(2,1)}) fusion(bf16[512,1,2,128]{3,0,2,1:T(8,128)(2,1)S(1)} %get-tuple-element.160, bf16[4,1024,1,128]{3,1,2,0:T(8,128)(2,1)} %get-tuple-element.159, s32[]{:T(128)} %get-tuple-element.147), kind=kOutput, calls=%fused_computation.3.clone.1 | convolution fusion | flops 272628736 | bytes 2626048 | tf_op jit(solution)/shard_map/while/body/eval_jaxpr/qhgd,khd->qhgk/dot_general | solution.py:67
  125.0 2.2 %fusion.71 = f32[512,1,2,128]{0,3,2,1:T(8,128)S(1)} fusion(bf16[1024,512,2]{1,0,2:T(8,128)(2,1)} %get-tuple-element.137, f32[512,1,2,128]{0,3,2,1:T(8,128)S(1)} %get-tuple-element.148, bf16[4,1024,1,128]{3,1,0,2:T(8,128)(2,1)} %get-tuple-element.158, s32[]{:T(128)} %get-tuple-element.147, pred[]{:T(512)S(6)} %compare.18), kind=kOutput, calls=%fused_computation.8.clone.1 | convolution fusion | flops 268697600 | bytes 3408385 | tf_op jit(solution)/shard_map/while/body/eval_jaxpr/qhgk,khd->qhgd/dot_general | solution.py:72
  127.2 3.1 %convert_reduce_fusion.2 = (f32[512,2]{0,1:T(2,128)S(1)}, bf16[1024,512,2]{1,0,2:T(8,128)(2,1)}) fusion(bf16[512,1,2,128]{3,0,2,1:T(8,128)(2,1)S(1)} %get-tuple-element.160, bf16[4,1024,1,128]{3,1,2,0:T(8,128)(2,1)} %get-tuple-element.159, s32[]{:T(128)} %get-tuple-element.147), kind=kOutput, calls=%fused_computation.3.clone.1 | convolution fusion | flops 272628736 | bytes 2626048 | tf_op jit(solution)/shard_map/while/body/eval_jaxpr/qhgd,khd->qhgk/dot_general | solution.py:67
  130.3 2.2 %fusion.71 = f32[512,1,2,128]{0,3,2,1:T(8,128)S(1)} fusion(bf16[1024,512,2]{1,0,2:T(8,128)(2,1)} %get-tuple-element.137, f32[512,1,2,128]{0,3,2,1:T(8,128)S(1)} %get-tuple-element.148, bf16[4,1024,1,128]{3,1,0,2:T(8,128)(2,1)} %get-tuple-element.158, s32[]{:T(128)} %get-tuple-element.147, pred[]{:T(512)S(6)} %compare.18), kind=kOutput, calls=%fused_computation.8.clone.1 | convolution fusion | flops 268697600 | bytes 3408385 | tf_op jit(solution)/shard_map/while/body/eval_jaxpr/qhgk,khd->qhgd/dot_general | solution.py:72
  132.6 0.1 divide_convert_fusion
  132.6 4.4 %fusion.18 = f32[512,512]{1,0:T(8,128)} fusion(bf16[512,2048]{1,0:T(8,128)(2,1)} %bitcast.18, bf16[1,2048,512]{2,1,0:T(8,128)(2,1)} %param.27), kind=kOutput, calls=%fused_computation.22 | convolution fusion | flops 1073741824 | bytes 5242880 | tf_op jit(solution)/shard_map/dot_general | solution.py:94
  137.1 6.2 %convolution_convert_fusion.1 = bf16[512,2048]{1,0:T(8,128)(2,1)} fusion(bf16[1,512,2048]{2,1,0:T(8,128)(2,1)S(1)} %copy-done, bf16[512,2048]{1,0:T(8,128)(2,1)} %bitcast.18, bf16[1,2048,512]{2,1,0:T(8,128)(2,1)} %param.28, f32[512,512]{1,0:T(8,128)} %fusion.18), kind=kOutput, calls=%fused_computation.18 | convolution fusion | flops 2150105088 | bytes 9437184 | tf_op jit(solution)/shard_map/dot_general | solution.py:97
  143.3 3.5 %all-to-all-start.1 = ((bf16[32,16,2048]{2,1,0:T(8,128)(2,1)}), bf16[32,16,2048]{2,1,0:T(8,128)(2,1)}, u32[]{:S(2)}, u32[]{:S(2)}) async-start(bf16[32,16,2048]{2,1,0:T(8,128)(2,1)} %bitcast.119), calls=%async_computation.2 | async-start | bytes 4194304 | tf_op jit(solution)/shard_map/all_to_all | solution.py:133
  146.8 0.3 reduce-scatter.2.cloned.1.call-start
  147.1 3.3 %convolution_convert_fusion = bf16[512,2048]{1,0:T(8,128)(2,1)} fusion(bf16[512,256]{0,1:T(8,128)(2,1)S(1)} %bitcast.121, bf16[1024,2048]{1,0:T(8,128)(2,1)} %param.21, s32[]{:T(128)S(6)} %select_n.58), kind=kOutput, calls=%fused_computation.17 | convolution fusion | flops 537919488 | bytes 3407876 | tf_op jit(solution)/shard_map/dot_general | solution.py:86
  150.4 0.7 copy-done.3
  151.1 0.1 copy.39
  151.2 44.4 %all-to-all-done.1 = bf16[32,16,2048]{2,1,0:T(8,128)(2,1)} async-done(((bf16[32,16,2048]{2,1,0:T(8,128)(2,1)}), bf16[32,16,2048]{2,1,0:T(8,128)(2,1)}, u32[]{:S(2)}, u32[]{:S(2)}) %all-to-all-start.1) | async-done | bytes 2097184 | tf_op jit(solution)/shard_map/all_to_all | solution.py:133
  195.6 4.2 %gather_fusion = bf16[256,2048]{1,0:T(8,128)(2,1)S(1)} fusion(bf16[512,2048]{1,0:T(8,128)(2,1)} %bitcast.23, s32[1024]{0:T(1024)S(1)} %pad_clamp_fusion), kind=kCustom, calls=%fused_computation.1 | custom fusion | bytes 2098176 | tf_op jit(solution)/shard_map/gather | solution.py:141
  199.8 2.3 %reshape.420 = f32[128,2,2048]{2,1,0:T(2,128)} reshape(bf16[256,2048]{1,0:T(8,128)(2,1)S(1)} %gather_fusion) | data formatting | bytes 3145728 | tf_op jit(solution)/shard_map/convert_element_type | solution.py:141
  202.2 5.6 %multiply_reduce_fusion = bf16[128,2048]{1,0:T(8,128)(2,1)} fusion(f32[128,2,2048]{2,1,0:T(2,128)} %reshape.420, f32[128,2]{1,0:T(8,128)S(1)} %copy.39), kind=kLoop, calls=%fused_computation.24 | loop fusion | flops 786432 | bytes 2622464 | tf_op jit(solution)/shard_map/reduce_sum | solution.py:143
  (45 shorter events, 0.5 us)
Async XLA Ops:
  7.2 129.9 %copy-start = (bf16[1,512,2048]{2,1,0:T(8,128)(2,1)S(1)}, bf16[1,512,2048]{2,1,0:T(8,128)(2,1)}, u32[]{:S(2)}) copy-start(bf16[1,512,2048]{2,1,0:T(8,128)(2,1)} %param.29) | copy-start | bytes 6291460
  7.2 4.1 %copy-start.5 = (s32[128,2]{0,1:T(2,128)S(1)}, s32[128,2]{0,1:T(2,128)}, u32[]{:S(2)}) copy-start(s32[128,2]{0,1:T(2,128)} %param.24) | copy-start | bytes 3076
  7.2 5.7 %copy-start.1 = (bf16[128,2048]{1,0:T(8,128)(2,1)S(1)}, bf16[128,2048]{1,0:T(8,128)(2,1)}, u32[]{:S(2)}) copy-start(bf16[128,2048]{1,0:T(8,128)(2,1)} %param.22) | copy-start | bytes 1572868
  7.2 6.0 %copy-start.4 = (f32[2048]{0:T(1024)S(1)}, f32[2048]{0:T(1024)}, u32[]{:S(2)}) copy-start(f32[2048]{0:T(1024)} %param.23) | copy-start | bytes 24580
  7.2 61.6 %all-gather.5.cloned.1.call-start = ((), (), s32[]{:S(2)}) async-start(), calls=%async_computation.4 | async-start | bytes 1179648 | tf_op jit(solution)/shard_map/all_gather | solution.py:55
  10.5 100.7 %all-gather.3.cloned.1.call-start = ((), (), s32[]{:S(2)}) async-start(), calls=%async_computation.3 | async-start | bytes 1179648 | tf_op jit(solution)/shard_map/all_gather | solution.py:56
  20.4 7.7 %copy-start.2 = (bf16[512,256]{1,0:T(8,128)(2,1)S(1)}, bf16[512,256]{1,0:T(8,128)(2,1)}, u32[]{:S(2)}) copy-start(bf16[512,256]{1,0:T(8,128)(2,1)} %param.16) | copy-start | bytes 786436
  20.4 8.4 %copy-start.7 = (f32[128]{0:T(128)S(1)}, f32[128]{0:T(128)}, u32[]{:S(2)}) copy-start(f32[128]{0:T(128)} %param.19) | copy-start | bytes 1540
  20.4 112.2 %all-to-all-start = ((bf16[32,16,2048]{2,1,0:T(8,128)(2,1)}), bf16[32,16,2048]{2,1,0:T(8,128)(2,1)}, u32[]{:S(2)}, u32[]{:S(2)}) async-start(bf16[32,16,2048]{2,1,0:T(8,128)(2,1)} %bitcast.118), calls=%async_computation.1 | async-start | bytes 4194304 | tf_op jit(solution)/shard_map/all_to_all | solution.py:123
  143.3 52.3 %all-to-all-start.1 = ((bf16[32,16,2048]{2,1,0:T(8,128)(2,1)}), bf16[32,16,2048]{2,1,0:T(8,128)(2,1)}, u32[]{:S(2)}, u32[]{:S(2)}) async-start(bf16[32,16,2048]{2,1,0:T(8,128)(2,1)} %bitcast.119), calls=%async_computation.2 | async-start | bytes 4194304 | tf_op jit(solution)/shard_map/all_to_all | solution.py:133
  146.8 61.0 %reduce-scatter.2.cloned.1.call-start = ((), (), s32[]{:S(2)}) async-start(), calls=%async_computation.5 | async-start | bytes 2621440 | tf_op jit(solution)/shard_map/reduce_scatter | solution.py:85
  150.4 0.7 copy-start.3
  150.4 0.7 copy-start.6
Sparse Core Ops, SparseCore 0:
  10.7 58.1 all-gather.4
  71.0 40.2 all-gather.2
  150.7 36.8 reduce-scatter.1
where the time goes:
time: 215 us; the launch traced here: 214 us
  waiting for transfers between devices  125 us (58%)
  matrix products  35.1 us (16%)
  local copies, waits for them, and re-layouts  18.9 us (9%)
  between operations  14 us (7%)
  starting transfers between devices  11.5 us (5%)
  other arithmetic  9.72 us (5%)
    all_to_all x1, waiting for transfers between devices, expert_half(): lax.all_to_all(expert_out.reshape(device_count, capacity, model_width), (...  44.4 us
    all_gather x1, waiting for transfers between devices, attention_half(): value_piece = lax.all_gather(values, 'ep', axis=0, tiled=True)  40.1 us
    all_gather x1, waiting for transfers between devices, attention_half(): key_piece = lax.all_gather(krot, 'ep', axis=0, tiled=True)  39.7 us
    dot_general x4, matrix products, key_step(): jnp.einsum('qhgd,khd->qhgk', qrot, key_tile, preferred_element_type=jnp.f...  12.4 us
    dot_general x4, matrix products, key_step(): jnp.einsum('qhgk,khd->qhgd', weights, value_tile, preferred_element_type=...  8.77 us
    all_to_all x1, starting transfers between devices, expert_half(): lax.all_to_all(sender.reshape(device_count, capacity, model_width), ('ep'...  7.63 us
    scatter x1, local copies, waits for them, and re-layouts, expert_half(): sender = jnp.zeros((device_count * capacity, model_width), jnp.bfloat16)....  7 us
    dot_general x1, matrix products, expert_apply(): jnp.dot(hidden, down_w, preferred_element_type=jnp.float32)  6.21 us
  transfers between devices with their start and end apart: 5, of which 3 were waited for; matrix products, arithmetic and copies ran while one was open for 23% of the time, Pallas kernels for 0%

commit v1 on v0

--- a/solution.py
+++ b/solution.py
@@ -52,8 +52,11 @@
         jnp.zeros((row_count, local_kv, group_size, head_dim), jnp.float32),
         jnp.zeros((row_count, local_kv, group_size), jnp.float32),
     )
-    key_piece = lax.all_gather(krot, "ep", axis=0, tiled=True)
-    value_piece = lax.all_gather(values, "ep", axis=0, tiled=True)
+    key_piece, value_piece = jnp.split(
+        lax.all_gather(jnp.concatenate([krot, values], 1), "ep", axis=0, tiled=True),
+        [krot.shape[1]],
+        1,
+    )
     piece_rows = key_piece.shape[0]
     key_block = math.gcd(piece_rows, 1024)
     block_count = piece_rows // key_block

time: 215 us -> 197 us (0.916)
  waiting for transfers between devices: 125 us -> 105 us
    all_gather x2 -> x1, waiting for transfers between devices: 79.8 us -> 60.9 us  [attention_half(): lax.all_gather(jnp.concatenate([krot, values], 1), 'ep', axis=0, tiled=True)]
    split x0 -> x1, local copies, waits for them, and re-layouts: none -> 3.02 us  [attention_half(): jnp.split(lax.all_gather(jnp.concatenate([krot, values], 1), 'ep', axis=0...]
    unnamed x21 -> x22, local copies, waits for them, and re-layouts: 4.54 us -> 2.27 us
  transfers between devices with their start and end apart: 5 -> 4, of which waited for: 3 -> 2; matrix products, arithmetic and copies ran while one was open for 23% -> 25% of each run, Pallas kernels for 0% -> 0%
where the time goes in v1:
time: 197 us; the launch traced here: 196 us
  waiting for transfers between devices  105 us (53%)
  matrix products  35.1 us (18%)
  local copies, waits for them, and re-layouts  19.9 us (10%)
  between operations  14.4 us (7%)
  starting transfers between devices  11.4 us (6%)
  other arithmetic  9.91 us (5%)
    all_gather x1, waiting for transfers between devices, attention_half(): lax.all_gather(jnp.concatenate([krot, values], 1), 'ep', axis=0, tiled=True)  60.9 us
    all_to_all x1, waiting for transfers between devices, expert_half(): lax.all_to_all(expert_out.reshape(device_count, capacity, model_width), (...  44.4 us
    dot_general x4, matrix products, key_step(): jnp.einsum('qhgd,khd->qhgk', qrot, key_tile, preferred_element_type=jnp.f...  12.4 us
    dot_general x4, matrix products, key_step(): jnp.einsum('qhgk,khd->qhgd', weights, value_tile, preferred_element_type=...  8.77 us
    all_to_all x1, starting transfers between devices, expert_half(): lax.all_to_all(sender.reshape(device_count, capacity, model_width), ('ep'...  7.63 us
    scatter x1, local copies, waits for them, and re-layouts, expert_half(): sender = jnp.zeros((device_count * capacity, model_width), jnp.bfloat16)....  7 us
    dot_general x1, matrix products, expert_apply(): jnp.dot(hidden, down_w, preferred_element_type=jnp.float32)  6.21 us
    reduce_sum x1, other arithmetic, expert_half(): return jnp.sum(picked * combine[:, :, None], axis=1).astype(jnp.bfloat16)  5.59 us
  transfers between devices with their start and end apart: 4, of which 2 were waited for; matrix products, arithmetic and copies ran while one was open for 25% of the time, Pallas kernels for 0%

profile of v1, /device:TPU:0, one launch (start us, length us, event | category | flops | bytes accessed | tf_op | source)
XLA Modules:
  0.0 196.2 jit_solution(18151817092221372603)
XLA Ops:
  7.3 1.2 copy.31
  8.5 0.7 fusion.40
  9.3 0.1 broadcast_multiply_fusion.1
  9.4 0.5 fusion.47
  9.9 0.1 copy.32
  10.0 0.1 copy.33
  10.1 0.9 pad_maximum_fusion
  11.0 0.1 copy.39
  11.1 0.1 eq.31
  11.3 0.1 eq.27
  11.4 0.6 reduce-window.6
  12.0 0.2 slice_reduce_fusion
  12.3 0.1 copy.38
  12.4 0.1 mul.229
  12.6 0.1 fusion.51
  12.7 0.2 fusion.26
  12.9 0.2 fusion.28
  13.1 7.0 %scatter_custom_fusion = bf16[512,2048]{1,0:T(8,128)(2,1)} fusion(s32[256]{0:T(256)S(1)} %bitcast.126, bf16[128,2048]{1,0:T(8,128)(2,1)S(1)} %fusion.28, s32[1024]{0:T(1024)S(1)} %pad_clamp_fusion.1, bf16[]{:T(256)} %constant.102.clone.1), kind=kCustom, calls=%fused_computation.32 | custom fusion | bytes 2097154 | tf_op jit(solution)/shard_map/scatter | solution.py:124
  20.1 7.6 %all-to-all-start = ((bf16[32,16,2048]{2,1,0:T(8,128)(2,1)}), bf16[32,16,2048]{2,1,0:T(8,128)(2,1)}, u32[]{:S(2)}, u32[]{:S(2)}) async-start(bf16[32,16,2048]{2,1,0:T(8,128)(2,1)} %bitcast.120), calls=%async_computation.1 | async-start | bytes 4194304 | tf_op jit(solution)/shard_map/all_to_all | solution.py:126
  27.7 0.1 copy.34
  27.9 0.5 fusion.44
  28.4 0.1 fusion.35
  28.5 0.1 fusion.36
  28.6 0.1 fusion.41
  28.7 0.2 copy.37
  28.9 60.9 %all-gather.2.cloned.1.call-done = bf16[4096,256]{1,0:T(8,128)(2,1)} async-done(((bf16[512,256]{1,0:T(8,128)(2,1)}), bf16[4096,256]{1,0:T(8,128)(2,1)}) %all-gather.2.cloned.1.call-update) | async-done | bytes 2097168 | tf_op jit(solution)/shard_map/all_gather | solution.py:56
  89.7 3.0 %fusion.63 = (bf16[4096,128]{1,0:T(8,128)(2,1)}, bf16[4096,128]{1,0:T(8,128)(2,1)}) fusion(bf16[4096,256]{1,0:T(8,128)(2,1)} %all-gather.2.cloned.1.call-done), kind=kLoop, calls=%fused_computation.106 | loop fusion | bytes 4194304 | tf_op jit(solution)/shard_map/split | solution.py:55
  92.8 21.3 %while.13 = (s32[]{:T(128)}, f32[512,1,2,128]{0,3,2,1:T(8,128)S(1)}, f32[512,1,2]{0,2,1:T(2,128)S(1)}, bf16[4,1024,1,128]{3,1,0,2:T(8,128)(2,1)}, bf16[4,1024,1,...) while((s32[]{:T(128)}, ...), condition=%wide.region_4.5_spmd.clone, body=%wide.region_2.4_spmd.clone.sunk | while | flops 541328384 | bytes 6046816 | solution.py:80
  92.8 3.1 %convert_reduce_fusion.2 = (f32[512,2]{0,1:T(2,128)S(1)}, bf16[1024,512,2]{1,0,2:T(8,128)(2,1)}) fusion(bf16[512,1,2,128]{3,0,2,1:T(8,128)(2,1)S(1)} %get-tuple-element.162, bf16[4,1024,1,128]{3,1,2,0:T(8,128)(2,1)} %get-tuple-element.161, s32[]{:T(128)} %get-tuple-element.149), kind=kOutput, calls=%fused_computation.3.clone.1 | convolution fusion | flops 272628736 | bytes 2626048 | tf_op jit(solution)/shard_map/while/body/eval_jaxpr/qhgd,khd->qhgk/dot_general | solution.py:70
  95.9 2.2 %fusion.72 = f32[512,1,2,128]{0,3,2,1:T(8,128)S(1)} fusion(bf16[1024,512,2]{1,0,2:T(8,128)(2,1)} %get-tuple-element.139, f32[512,1,2,128]{0,3,2,1:T(8,128)S(1)} %get-tuple-element.150, bf16[4,1024,1,128]{3,1,0,2:T(8,128)(2,1)} %get-tuple-element.160, s32[]{:T(128)} %get-tuple-element.149, pred[]{:T(512)S(6)} %compare.18), kind=kOutput, calls=%fused_computation.8.clone.1 | convolution fusion | flops 268697600 | bytes 3408385 | tf_op jit(solution)/shard_map/while/body/eval_jaxpr/qhgk,khd->qhgd/dot_general | solution.py:75
  98.1 3.1 %convert_reduce_fusion.2 = (f32[512,2]{0,1:T(2,128)S(1)}, bf16[1024,512,2]{1,0,2:T(8,128)(2,1)}) fusion(bf16[512,1,2,128]{3,0,2,1:T(8,128)(2,1)S(1)} %get-tuple-element.162, bf16[4,1024,1,128]{3,1,2,0:T(8,128)(2,1)} %get-tuple-element.161, s32[]{:T(128)} %get-tuple-element.149), kind=kOutput, calls=%fused_computation.3.clone.1 | convolution fusion | flops 272628736 | bytes 2626048 | tf_op jit(solution)/shard_map/while/body/eval_jaxpr/qhgd,khd->qhgk/dot_general | solution.py:70
  101.2 2.2 %fusion.72 = f32[512,1,2,128]{0,3,2,1:T(8,128)S(1)} fusion(bf16[1024,512,2]{1,0,2:T(8,128)(2,1)} %get-tuple-element.139, f32[512,1,2,128]{0,3,2,1:T(8,128)S(1)} %get-tuple-element.150, bf16[4,1024,1,128]{3,1,0,2:T(8,128)(2,1)} %get-tuple-element.160, s32[]{:T(128)} %get-tuple-element.149, pred[]{:T(512)S(6)} %compare.18), kind=kOutput, calls=%fused_computation.8.clone.1 | convolution fusion | flops 268697600 | bytes 3408385 | tf_op jit(solution)/shard_map/while/body/eval_jaxpr/qhgk,khd->qhgd/dot_general | solution.py:75
  103.4 3.1 %convert_reduce_fusion.2 = (f32[512,2]{0,1:T(2,128)S(1)}, bf16[1024,512,2]{1,0,2:T(8,128)(2,1)}) fusion(bf16[512,1,2,128]{3,0,2,1:T(8,128)(2,1)S(1)} %get-tuple-element.162, bf16[4,1024,1,128]{3,1,2,0:T(8,128)(2,1)} %get-tuple-element.161, s32[]{:T(128)} %get-tuple-element.149), kind=kOutput, calls=%fused_computation.3.clone.1 | convolution fusion | flops 272628736 | bytes 2626048 | tf_op jit(solution)/shard_map/while/body/eval_jaxpr/qhgd,khd->qhgk/dot_general | solution.py:70
  106.5 2.2 %fusion.72 = f32[512,1,2,128]{0,3,2,1:T(8,128)S(1)} fusion(bf16[1024,512,2]{1,0,2:T(8,128)(2,1)} %get-tuple-element.139, f32[512,1,2,128]{0,3,2,1:T(8,128)S(1)} %get-tuple-element.150, bf16[4,1024,1,128]{3,1,0,2:T(8,128)(2,1)} %get-tuple-element.160, s32[]{:T(128)} %get-tuple-element.149, pred[]{:T(512)S(6)} %compare.18), kind=kOutput, calls=%fused_computation.8.clone.1 | convolution fusion | flops 268697600 | bytes 3408385 | tf_op jit(solution)/shard_map/while/body/eval_jaxpr/qhgk,khd->qhgd/dot_general | solution.py:75
  108.8 3.1 %convert_reduce_fusion.2 = (f32[512,2]{0,1:T(2,128)S(1)}, bf16[1024,512,2]{1,0,2:T(8,128)(2,1)}) fusion(bf16[512,1,2,128]{3,0,2,1:T(8,128)(2,1)S(1)} %get-tuple-element.162, bf16[4,1024,1,128]{3,1,2,0:T(8,128)(2,1)} %get-tuple-element.161, s32[]{:T(128)} %get-tuple-element.149), kind=kOutput, calls=%fused_computation.3.clone.1 | convolution fusion | flops 272628736 | bytes 2626048 | tf_op jit(solution)/shard_map/while/body/eval_jaxpr/qhgd,khd->qhgk/dot_general | solution.py:70
  111.9 2.2 %fusion.72 = f32[512,1,2,128]{0,3,2,1:T(8,128)S(1)} fusion(bf16[1024,512,2]{1,0,2:T(8,128)(2,1)} %get-tuple-element.139, f32[512,1,2,128]{0,3,2,1:T(8,128)S(1)} %get-tuple-element.150, bf16[4,1024,1,128]{3,1,0,2:T(8,128)(2,1)} %get-tuple-element.160, s32[]{:T(128)} %get-tuple-element.149, pred[]{:T(512)S(6)} %compare.18), kind=kOutput, calls=%fused_computation.8.clone.1 | convolution fusion | flops 268697600 | bytes 3408385 | tf_op jit(solution)/shard_map/while/body/eval_jaxpr/qhgk,khd->qhgd/dot_general | solution.py:75
  114.1 0.1 divide_convert_fusion
  114.2 4.4 %fusion.18 = f32[512,512]{1,0:T(8,128)} fusion(bf16[512,2048]{1,0:T(8,128)(2,1)} %bitcast.19, bf16[1,2048,512]{2,1,0:T(8,128)(2,1)} %param.27), kind=kOutput, calls=%fused_computation.22 | convolution fusion | flops 1073741824 | bytes 5242880 | tf_op jit(solution)/shard_map/dot_general | solution.py:97
  118.6 6.2 %convolution_convert_fusion.1 = bf16[512,2048]{1,0:T(8,128)(2,1)} fusion(bf16[1,512,2048]{2,1,0:T(8,128)(2,1)S(1)} %copy-done, bf16[512,2048]{1,0:T(8,128)(2,1)} %bitcast.19, bf16[1,2048,512]{2,1,0:T(8,128)(2,1)} %param.28, f32[512,512]{1,0:T(8,128)} %fusion.18), kind=kOutput, calls=%fused_computation.18 | convolution fusion | flops 2150105088 | bytes 9437184 | tf_op jit(solution)/shard_map/dot_general | solution.py:100
  124.8 3.5 %all-to-all-start.1 = ((bf16[32,16,2048]{2,1,0:T(8,128)(2,1)}), bf16[32,16,2048]{2,1,0:T(8,128)(2,1)}, u32[]{:S(2)}, u32[]{:S(2)}) async-start(bf16[32,16,2048]{2,1,0:T(8,128)(2,1)} %bitcast.122), calls=%async_computation.2 | async-start | bytes 4194304 | tf_op jit(solution)/shard_map/all_to_all | solution.py:136
  128.3 0.3 reduce-scatter.2.cloned.1.call-start
  128.6 3.3 %convolution_convert_fusion = bf16[512,2048]{1,0:T(8,128)(2,1)} fusion(bf16[512,256]{0,1:T(8,128)(2,1)S(1)} %bitcast.123, bf16[1024,2048]{1,0:T(8,128)(2,1)} %param.21, s32[]{:T(128)S(6)} %select_n.58), kind=kOutput, calls=%fused_computation.17 | convolution fusion | flops 537919488 | bytes 3407876 | tf_op jit(solution)/shard_map/dot_general | solution.py:89
  131.9 0.7 copy-done.4
  132.7 0.1 copy.42
  132.8 44.4 %all-to-all-done.1 = bf16[32,16,2048]{2,1,0:T(8,128)(2,1)} async-done(((bf16[32,16,2048]{2,1,0:T(8,128)(2,1)}), bf16[32,16,2048]{2,1,0:T(8,128)(2,1)}, u32[]{:S(2)}, u32[]{:S(2)}) %all-to-all-start.1) | async-done | bytes 2097184 | tf_op jit(solution)/shard_map/all_to_all | solution.py:136
  177.2 4.2 %gather_fusion = bf16[256,2048]{1,0:T(8,128)(2,1)S(1)} fusion(bf16[512,2048]{1,0:T(8,128)(2,1)} %bitcast.24, s32[1024]{0:T(1024)S(1)} %pad_clamp_fusion), kind=kCustom, calls=%fused_computation.1 | custom fusion | bytes 2098176 | tf_op jit(solution)/shard_map/gather | solution.py:144
  181.4 2.3 %reshape.420 = f32[128,2,2048]{2,1,0:T(2,128)} reshape(bf16[256,2048]{1,0:T(8,128)(2,1)S(1)} %gather_fusion) | data formatting | bytes 3145728 | tf_op jit(solution)/shard_map/convert_element_type | solution.py:144
  183.8 5.6 %multiply_reduce_fusion = bf16[128,2048]{1,0:T(8,128)(2,1)} fusion(f32[128,2,2048]{2,1,0:T(2,128)} %reshape.420, f32[128,2]{1,0:T(8,128)S(1)} %copy.42), kind=kLoop, calls=%fused_computation.24 | loop fusion | flops 786432 | bytes 2622464 | tf_op jit(solution)/shard_map/reduce_sum | solution.py:146
  (46 shorter events, 0.4 us)
Async XLA Ops:
  7.2 111.4 %copy-start = (bf16[1,512,2048]{2,1,0:T(8,128)(2,1)S(1)}, bf16[1,512,2048]{2,1,0:T(8,128)(2,1)}, u32[]{:S(2)}) copy-start(bf16[1,512,2048]{2,1,0:T(8,128)(2,1)} %param.29) | copy-start | bytes 6291460
  7.2 2.9 %copy-start.3 = (bf16[512,128]{1,0:T(8,128)(2,1)S(1)}, bf16[512,128]{1,0:T(8,128)(2,1)}, u32[]{:S(2)}) copy-start(bf16[512,128]{1,0:T(8,128)(2,1)} %param.18) | copy-start | bytes 393220
  7.2 3.8 %copy-start.6 = (s32[128,2]{0,1:T(2,128)S(1)}, s32[128,2]{0,1:T(2,128)}, u32[]{:S(2)}) copy-start(s32[128,2]{0,1:T(2,128)} %param.24) | copy-start | bytes 3076
  7.2 5.5 %copy-start.1 = (bf16[128,2048]{1,0:T(8,128)(2,1)S(1)}, bf16[128,2048]{1,0:T(8,128)(2,1)}, u32[]{:S(2)}) copy-start(bf16[128,2048]{1,0:T(8,128)(2,1)} %param.22) | copy-start | bytes 1572868
  7.2 5.7 %copy-start.5 = (f32[2048]{0:T(1024)S(1)}, f32[2048]{0:T(1024)}, u32[]{:S(2)}) copy-start(f32[2048]{0:T(1024)} %param.23) | copy-start | bytes 24580
  7.2 82.5 %all-gather.2.cloned.1.call-start = ((), (), s32[]{:S(2)}) async-start(), calls=%async_computation.3 | async-start | bytes 2359296 | tf_op jit(solution)/shard_map/all_gather | solution.py:56
  20.1 7.7 %copy-start.2 = (bf16[512,256]{1,0:T(8,128)(2,1)S(1)}, bf16[512,256]{1,0:T(8,128)(2,1)}, u32[]{:S(2)}) copy-start(bf16[512,256]{1,0:T(8,128)(2,1)} %param.16) | copy-start | bytes 786436
  20.1 8.4 %copy-start.8 = (f32[128]{0:T(128)S(1)}, f32[128]{0:T(128)}, u32[]{:S(2)}) copy-start(f32[128]{0:T(128)} %param.19) | copy-start | bytes 1540
  20.1 94.1 %all-to-all-start = ((bf16[32,16,2048]{2,1,0:T(8,128)(2,1)}), bf16[32,16,2048]{2,1,0:T(8,128)(2,1)}, u32[]{:S(2)}, u32[]{:S(2)}) async-start(bf16[32,16,2048]{2,1,0:T(8,128)(2,1)} %bitcast.120), calls=%async_computation.1 | async-start | bytes 4194304 | tf_op jit(solution)/shard_map/all_to_all | solution.py:126
  124.8 52.4 %all-to-all-start.1 = ((bf16[32,16,2048]{2,1,0:T(8,128)(2,1)}), bf16[32,16,2048]{2,1,0:T(8,128)(2,1)}, u32[]{:S(2)}, u32[]{:S(2)}) async-start(bf16[32,16,2048]{2,1,0:T(8,128)(2,1)} %bitcast.122), calls=%async_computation.2 | async-start | bytes 4194304 | tf_op jit(solution)/shard_map/all_to_all | solution.py:136
  128.3 61.0 %reduce-scatter.2.cloned.1.call-start = ((), (), s32[]{:S(2)}) async-start(), calls=%async_computation.4 | async-start | bytes 2621440 | tf_op jit(solution)/shard_map/reduce_scatter | solution.py:88
  131.9 0.7 copy-start.4
  131.9 0.7 copy-start.7
Sparse Core Ops, SparseCore 0:
  11.1 78.5 all-gather.1
  132.2 36.7 reduce-scatter.1
